TPU v7x, 32 devices: a whole 2x2x4 slice. The times are simulated.
32 devices in a mesh: sp: 8 (over z, core), tp: 4 (over y, x).
Axes of the slice: x: 2, y: 2, z: 4, core: 2. Of those that a mesh axis runs over, the one named last changes fastest.
Arguments:
- tokens: bfloat16 [1536, 4096], P('sp', 'tp'), may hold values from -60 to 60
- lean_query: bfloat16 [1536, 16, 64], P('sp', 'tp'), may hold values from -6 to 6
- lean_key: bfloat16 [1536, 2, 64], P('sp'), may hold values from -6 to 6
- lean_value: bfloat16 [1536, 2, 64], P('sp'), may hold values from -6 to 6
- lean_gains: float32 [2, 64], replicated, may hold values from 0.25 to 7.5
- broad_query: bfloat16 [1536, 16, 128], P('sp', 'tp'), may hold values from -6 to 6
- broad_key: bfloat16 [1536, 2, 128], P('sp'), may hold values from -6 to 6
- broad_value: bfloat16 [1536, 2, 128], P('sp'), may hold values from -6 to 6
- broad_gains: float32 [2, 128], replicated, may hold values from 0.25 to 7.5
- mixer_gain: float32 [3072], replicated, may hold values from 0.1 to 1.9
- output_weight: bfloat16 [3072, 4096], P(None, 'tp'), may hold values from -0.109375 to 0.109375
- channel_gain: float32 [4096], P('tp'), may hold values from 0.1 to 1.9
- gate_weight: bfloat16 [8, 4096, 2048], P('sp', None, 'tp'), may hold values from -0.09375 to 0.09375
- up_weight: bfloat16 [8, 4096, 2048], P('sp', None, 'tp'), may hold values from -0.09375 to 0.09375
- down_weight: bfloat16 [8, 2048, 4096], P('sp', None, 'tp'), may hold values from -0.125 to 0.125
- route_experts: int32 [1536, 2], P('sp'), may hold values from 0 to 7, as said below
- route_logits: float32 [1536, 2], P('sp'), may hold values from -6 to 6
- group_weight: float32 [1536], P('sp'), may hold values from 0.3 to 1
Outputs:
- encoded: bfloat16 [1536, 4096], P('sp', 'tp')
Inputs may be any that keep to these rules, and one draw needn't show every extreme that they name: `route_experts`: each row names two different experts of one group, expert e lying in group e // 2. In every aligned block of 192 rows no expert is named by more than 96 rows; one group, the same for all blocks, is named by exactly half of each block's rows, and each of its experts by exactly 96 of them.
All inputs are finite; a program needn't handle non-finite values.
Results may differ from a plain program's by a relative error of at most 0.0083.
Values may be sent and summed in bfloat16 or wider, within the bound.
A program may use at most 64 MiB of HBM per device.

v0:
```python
import functools

import jax
import jax.numpy as jnp
import numpy as np
from jax import lax
from jax.experimental import pallas as pl
from jax.experimental.pallas import tpu as pltpu
from jax.sharding import PartitionSpec as P

D = 4096
HQ_A = 16
KV_A = 2
HQ_B = 16
KV_B = 2
GRID_W = 64
GROUPS = 4


epsilon = 1e-06
theta_base = 10000.0
floor_score = -1e30


def axial_angles(positions, head_size):
    quarter = head_size // 4
    frequency = theta_base ** (-jnp.arange(quarter, dtype=jnp.float32) / quarter)
    grid_rows = (positions // GRID_W).astype(jnp.float32)
    grid_columns = (positions % GRID_W).astype(jnp.float32)
    return (grid_rows[:, None] * frequency[None, :], grid_columns[:, None] * frequency[None, :])


def turn_half(values, angles):
    half_width = values.shape[-1] // 2
    first_half = values[..., :half_width]
    second = values[..., half_width:]
    cosine = jnp.cos(angles)[:, None, :]
    sine_part = jnp.sin(angles)[:, None, :]
    return jnp.concatenate(
        [first_half * cosine - second * sine_part, second * cosine + first_half * sine_part],
        axis=-1,
    )


def prepare(raw_values, gain_row, positions):
    values = raw_values.astype(jnp.float32)
    values = (
        values * lax.rsqrt(jnp.mean(values * values, axis=-1, keepdims=True) + epsilon) * gain_row
    )
    row_angles, column_angles = axial_angles(positions, raw_values.shape[-1])
    half_width = raw_values.shape[-1] // 2
    turned = jnp.concatenate(
        [
            turn_half(values[..., :half_width], row_angles),
            turn_half(values[..., half_width:], column_angles),
        ],
        axis=-1,
    )
    return turned.astype(jnp.bfloat16)


def group_norm(head_rows, gain_row):
    values = head_rows.astype(jnp.float32)
    return (
        values * lax.rsqrt(jnp.mean(values * values, axis=-1, keepdims=True) + epsilon) * gain_row
    ).astype(jnp.bfloat16)


def own_heads(query_raw, key_raw, value_raw, gain_pair, positions, lane_index, group_ratio):
    head_count, head_size = (query_raw.shape[1], query_raw.shape[2])
    key_heads = max(1, head_count // group_ratio)
    kv_start = lane_index * head_count // group_ratio
    key_part = lax.dynamic_slice_in_dim(key_raw, kv_start, key_heads, 1)
    value_part = lax.dynamic_slice_in_dim(value_raw, kv_start, key_heads, 1)
    queries = prepare(query_raw, gain_pair[0], positions).reshape(
        query_raw.shape[0], key_heads, head_count // key_heads, head_size
    )
    return (queries, prepare(key_part, gain_pair[1], positions), value_part)


def start_state(queries):
    row_count = queries.shape[0]
    head_count = queries.shape[1] * queries.shape[2]
    return (
        jnp.full((head_count, row_count), floor_score, jnp.float32),
        jnp.zeros((head_count, row_count), jnp.float32),
        jnp.zeros((row_count, head_count, queries.shape[3]), jnp.float32),
    )


def attend_piece(fold_state, queries, keys, values):
    peak_score, weight_sum, accumulated = fold_state
    row_count, key_heads, grouped, head_size = queries.shape
    key_count = keys.shape[0]
    scores = jnp.einsum(
        "qkgd,skd->kgqs", queries, keys, preferred_element_type=jnp.float32
    ) * head_size ** (-0.5)
    scores = scores.reshape(key_heads * grouped, row_count, key_count)
    new_peak = jnp.maximum(peak_score, jnp.max(scores, axis=-1))
    weights = jnp.exp(scores - new_peak[..., None])
    new_sum = jnp.sum(weights, axis=-1)
    rounded = weights.astype(jnp.bfloat16).reshape(key_heads, grouped, row_count, key_count)
    partial_value = jnp.einsum(
        "kgqs,skd->qkgd", rounded, values, preferred_element_type=jnp.float32
    )
    partial_value = partial_value.reshape(row_count, key_heads * grouped, head_size)
    return (new_peak, new_sum, partial_value)


def finish_heads(fold_state):
    accumulated = fold_state[2]
    return (
        (accumulated / jnp.transpose(fold_state[1])[:, :, None])
        .astype(jnp.bfloat16)
        .reshape(accumulated.shape[0], -1)
    )


MESH = pl.DeviceIdType.MESH
EXTRA = 128


def enter(peers):
    barrier = pltpu.get_barrier_semaphore()
    for peer in peers:
        pl.semaphore_signal(barrier, inc=1, device_id=peer, device_id_type=MESH)
    pl.semaphore_wait(barrier, len(peers))


def place():
    sp, tp = lax.axis_index("sp"), lax.axis_index("tp")
    z, core = sp // 2, sp % 2
    y, x = tp // 2, tp % 2
    sibling = {"sp": z * 2 + (1 - core), "tp": tp}
    x_peer = {"sp": sp, "tp": y * 2 + (1 - x)}
    y_peer = {"sp": sp, "tp": (1 - y) * 2 + x}
    chunks = (tp, y * 2 + (1 - x), (1 - y) * 2 + x, (1 - y) * 2 + (1 - x))
    return z, core, tp, sibling, x_peer, y_peer, chunks


def remote(source, target, send_sem, recv_sem, device):
    return pltpu.make_async_remote_copy(
        src_ref=source,
        dst_ref=target,
        send_sem=send_sem,
        recv_sem=recv_sem,
        device_id=device,
        device_id_type=MESH,
    )


def front_kernel(
    chips,
    lean_q,
    lean_k,
    lean_v,
    broad_q,
    broad_k,
    broad_v,
    lean_gain,
    broad_gain,
    cosines,
    sines,
    mixer_gain,
    tokens,
    channel_gain,
    picker,
    route_columns,
    weight_hbm,
    stream_out,
    going_out,
    own,
    keys,
    queries,
    peak,
    total,
    mass,
    lean_heads,
    broad_heads,
    weight,
    lean_acc,
    broad_acc,
    w_sem,
    k_send,
    k_recv,
    h_send,
    h_recv,
):
    z, core, tp, sibling, x_peer, y_peer, chunks = place()
    x, y = tp % 2, tp // 2
    rows = own.shape[0]
    half = rows // 2
    lanes = 128
    peers = [{"sp": ((z + d) % chips) * 2 + core, "tp": tp} for d in range(1, chips)]
    load = pltpu.make_async_copy(weight_hbm, weight, w_sem.at[0])
    load.start()
    lane = lax.broadcasted_iota(jnp.int32, (rows, lanes), 1)
    low = lane < lanes // 2

    def turned(raw, gain, size):
        values = raw.astype(jnp.float32)
        squares = values * values
        if size == lanes:
            mean = jnp.sum(squares, axis=1, keepdims=True) / size
        else:
            first = jnp.sum(jnp.where(low, squares, 0.0), axis=1, keepdims=True)
            second = jnp.sum(jnp.where(low, 0.0, squares), axis=1, keepdims=True)
            mean = jnp.where(low, first, second) / size
        values = values * lax.rsqrt(mean + epsilon) * gain
        quarter = size // 4
        partner = jnp.where(
            lane % (2 * quarter) < quarter,
            pltpu.roll(values, lanes - quarter, 1),
            pltpu.roll(values, quarter, 1),
        )
        part = pl.ds(0 if size == lanes else lanes, lanes)
        return values * cosines[:, part] + partner * sines[:, part]

    def swapped(values):
        return pltpu.roll(values, lanes // 2, 1)

    key_columns = pl.ds(pl.multiple_of(y * lanes, lanes), lanes)
    own[:, :lanes] = turned(broad_k[:, key_columns], broad_gain[1:2, :], lanes).astype(jnp.bfloat16)
    own[:, lanes : 2 * lanes] = broad_v[:, key_columns]
    both_keys = turned(lean_k[...], lean_gain[1:2, :], lanes // 2)
    both_values = lean_v[...].astype(jnp.float32)
    at_first = (1 - y).astype(jnp.float32)
    lean_key = both_keys * at_first + swapped(both_keys) * (1.0 - at_first)
    lean_value = swapped(both_values) * at_first + both_values * (1.0 - at_first)
    own[:, 2 * lanes :] = jnp.where(low, lean_key, lean_value).astype(jnp.bfloat16)

    enter(peers + [sibling, x_peer, y_peer])
    pending = []
    arrivals = {}

    def send(kind, d, source, target, device):
        copy = remote(source, target, k_send.at[kind, d], k_recv.at[kind, d], device)
        copy.start()
        pending.append(copy)
        arrivals[kind, d] = copy

    mine = pl.ds(pl.multiple_of(x * half, half), half)
    other = pl.ds(pl.multiple_of((1 - x) * half, half), half)
    side_mine = pl.ds(pl.multiple_of(rows + x * half, half), half)
    side_other = pl.ds(pl.multiple_of(rows + (1 - x) * half, half), half)
    Z, X, A, B = 0, 1, 2, 3
    for d in range(1, chips):
        send(Z, d, own.at[mine], keys.at[d, mine], peers[d - 1])
    send(A, 0, own, keys.at[0, pl.ds(rows, rows)], sibling)
    keys[0, pl.ds(0, rows)] = own[...]

    heads = queries.shape[1]
    for h in range(heads):
        part = pl.ds(h * lanes, lanes)
        queries[1, h] = turned(broad_q[:, part], broad_gain[0:1, :], lanes).astype(jnp.bfloat16)
    for h in range(heads // 2):
        part = pl.ds(h * lanes, lanes)
        pair = turned(lean_q[:, part], lean_gain[0:1, :], lanes // 2)
        queries[0, 2 * h] = jnp.where(low, pair, 0.0).astype(jnp.bfloat16)
        queries[0, 2 * h + 1] = jnp.where(low, swapped(pair), 0.0).astype(jnp.bfloat16)

    def attend(d, kind):
        size = lanes // 2 if kind == 0 else lanes
        key_part = pl.ds(2 * lanes, lanes) if kind == 0 else pl.ds(0, lanes)
        value_part = pl.ds(2 * lanes, lanes) if kind == 0 else pl.ds(lanes, lanes)

        def one_head(h, carry):
            scores = lax.dot_general(
                queries[kind, h],
                keys[d, :, key_part],
                (((1,), (1,)), ((), ())),
                preferred_element_type=jnp.float32,
            ) * (size**-0.5)
            top = jnp.max(scores, axis=1, keepdims=True)
            if d:
                old = peak[kind, h][:, :1]
                top = jnp.maximum(old, top)
            weights = jnp.exp(scores - top)
            summed = jnp.sum(weights, axis=1, keepdims=True)
            partial = jnp.dot(
                weights.astype(jnp.bfloat16),
                keys[d, :, value_part],
                preferred_element_type=jnp.float32,
            )
            if d:
                shrink = jnp.exp(old - top)
                summed = summed + total[kind, h][:, :1] * shrink
                partial = partial + mass[kind, h] * shrink
            peak[kind, h] = jnp.broadcast_to(top, (rows, lanes))
            total[kind, h] = jnp.broadcast_to(summed, (rows, lanes))
            mass[kind, h] = partial
            return carry

        lax.fori_loop(0, heads, one_head, 0)

    def forward(d):
        arrivals[Z, d].wait_recv()
        send(X, d, keys.at[d, mine], keys.at[d, mine], x_peer)
        send(A, d, keys.at[d, mine], keys.at[d, side_mine], sibling)

    def forward_other(d):
        arrivals[X, d].wait_recv()
        send(B, d, keys.at[d, other], keys.at[d, side_other], sibling)

    forward(1)
    arrivals[A, 0].wait_recv()
    attend(0, 0)
    forward_other(1)
    attend(0, 1)
    for d in range(1, chips):
        if d + 1 < chips:
            forward(d + 1)
        arrivals[A, d].wait_recv()
        arrivals[B, d].wait_recv()
        if d + 1 < chips:
            attend(d, 0)
            forward_other(d + 1)
            attend(d, 1)

    gathers = {}

    def spread(kind, buffer):
        for k, peer in ((0, x_peer), (1, y_peer)):
            n = kind * 4 + k
            copy = remote(buffer.at[0], buffer.at[1 + k], h_send.at[n], h_recv.at[n], peer)
            copy.start()
            pending.append(copy)
            gathers[kind, k] = copy

    def relay(kind, buffer):
        for k, peer in ((0, y_peer), (1, x_peer)):
            n = kind * 4 + 2 + k
            gathers[kind, k].wait_recv()
            part = pl.ds(k * half, half)
            copy = remote(
                buffer.at[1 + k, part], buffer.at[3, part], h_send.at[n], h_recv.at[n], peer
            )
            copy.start()
            pending.append(copy)
            gathers[kind, 2 + k] = copy

    def finished(kind, h):
        return mass[kind, h] / total[kind, h]

    attend(chips - 1, 0)
    for h in range(heads // 2):
        pair = jnp.where(low, swapped(finished(0, 2 * h)), finished(0, 2 * h + 1))
        lean_heads[0, :, pl.ds(h * lanes, lanes)] = pair.astype(jnp.bfloat16)
    spread(0, lean_heads)
    attend(chips - 1, 1)
    for h in range(heads):
        broad_heads[0, :, pl.ds(h * lanes, lanes)] = finished(1, h).astype(jnp.bfloat16)
    spread(1, broad_heads)
    load.wait()
    lean_width, broad_width = lean_heads.shape[2], broad_heads.shape[2]
    squares = [0.0, 0.0]

    def project(kind, r):
        buffer, acc, width, start = (
            (lean_heads, lean_acc, lean_width, 0),
            (broad_heads, broad_acc, broad_width, 4 * lean_width),
        )[kind]
        part = pl.ds(pl.multiple_of(start + chunks[r] * width, width), width)
        values = buffer[r].astype(jnp.float32)
        squares[kind] = squares[kind] + jnp.sum(values * values, axis=1, keepdims=True)
        scaled = (values * mixer_gain[:, part]).astype(jnp.bfloat16)
        product = jnp.dot(scaled, weight[part, :], preferred_element_type=jnp.float32)
        if r == 0:
            acc[...] = product
        else:
            acc[...] += product

    project(0, 0)
    relay(0, lean_heads)
    project(1, 0)
    project(0, 1)
    project(0, 2)
    relay(1, broad_heads)
    project(1, 1)
    project(1, 2)
    for kind in (0, 1):
        gathers[kind, 2].wait_recv()
        gathers[kind, 3].wait_recv()
        project(kind, 3)
    lean_scale = lax.rsqrt(squares[0] / (4 * lean_width) + epsilon)
    broad_scale = lax.rsqrt(squares[1] / (4 * broad_width) + epsilon)
    stream = (
        tokens[...].astype(jnp.float32)
        + lean_acc[...] * lean_scale
        + broad_acc[...] * broad_scale
    )
    stream_out[...] = stream
    width = stream.shape[1]
    norm = jnp.sum(stream * stream, axis=1, keepdims=True)
    norm_high = norm.astype(jnp.bfloat16).astype(jnp.float32)
    extra = jnp.where(
        lane == 0, norm_high, jnp.where(lane == 1, norm - norm_high, route_columns[...])
    ).astype(jnp.bfloat16)
    scaled = (stream * channel_gain[...]).astype(jnp.bfloat16)
    going_out[:, :width] = jnp.dot(
        picker[...], scaled, preferred_element_type=jnp.float32
    ).astype(jnp.bfloat16)
    going_out[:, width:] = jnp.dot(
        picker[...], extra, preferred_element_type=jnp.float32
    ).astype(jnp.bfloat16)
    for copy in pending:
        copy.wait_send()


def lane_frequencies(head_size):
    quarter = head_size // 4
    lane = np.arange(128) % head_size
    frequency = theta_base ** (-(lane % quarter).astype(np.float32) / np.float32(quarter))
    by_row = lane < head_size // 2
    sign = np.where(lane // quarter % 2 == 0, -1.0, 1.0)
    return frequency.astype(np.float32), by_row, sign.astype(np.float32)


def run_front(
    chips,
    positions,
    lean,
    broad,
    lean_gains,
    broad_gains,
    mixer_gain,
    tokens,
    channel_gain,
    picker,
    route_columns,
    output_weight,
):
    rows, width = tokens.shape
    heads = lean[0].shape[1]
    tables = [lane_frequencies(part[0].shape[2]) for part in (broad, lean)]
    frequency, by_row, sign = (np.concatenate(parts)[None, :] for parts in zip(*tables))
    row = (positions // GRID_W).astype(jnp.float32)[:, None]
    column = (positions % GRID_W).astype(jnp.float32)[:, None]
    angles = jnp.where(by_row, row, column) * frequency
    flat = [part.reshape(rows, -1) for part in lean + broad]
    return pl.pallas_call(
        functools.partial(front_kernel, chips),
        out_shape=[
            jax.ShapeDtypeStruct((rows, width), jnp.float32),
            jax.ShapeDtypeStruct((picker.shape[0], width + EXTRA), jnp.bfloat16),
        ],
        in_specs=[pl.BlockSpec(memory_space=pltpu.VMEM)] * 15
        + [pl.BlockSpec(memory_space=pl.ANY)],
        out_specs=[pl.BlockSpec(memory_space=pltpu.VMEM)] * 2,
        scratch_shapes=[
            pltpu.VMEM((rows, 384), jnp.bfloat16),
            pltpu.VMEM((chips, 2 * rows, 384), jnp.bfloat16),
            pltpu.VMEM((2, heads, rows, 128), jnp.bfloat16),
            pltpu.VMEM((2, heads, rows, 128), jnp.float32),
            pltpu.VMEM((2, heads, rows, 128), jnp.float32),
            pltpu.VMEM((2, heads, rows, 128), jnp.float32),
            pltpu.VMEM((4, rows, heads * 64), jnp.bfloat16),
            pltpu.VMEM((4, rows, heads * 128), jnp.bfloat16),
            pltpu.VMEM(output_weight.shape, jnp.bfloat16),
            pltpu.VMEM((rows, width), jnp.float32),
            pltpu.VMEM((rows, width), jnp.float32),
            pltpu.SemaphoreType.DMA((1,)),
            pltpu.SemaphoreType.DMA((4, chips)),
            pltpu.SemaphoreType.DMA((4, chips)),
            pltpu.SemaphoreType.DMA((8,)),
            pltpu.SemaphoreType.DMA((8,)),
        ],
        compiler_params=pltpu.CompilerParams(
            collective_id=0, has_side_effects=True, vmem_limit_bytes=48 * 1024 * 1024
        ),
    )(
        *flat,
        jnp.concatenate([lean_gains, lean_gains], axis=1),
        broad_gains,
        jnp.cos(angles),
        jnp.sin(angles) * sign,
        mixer_gain[None, :],
        tokens,
        channel_gain[None, :],
        picker,
        route_columns,
        output_weight,
    )


def experts_kernel(
    width,
    out_going,
    gate_hbm,
    up_hbm,
    down_hbm,
    out_ref,
    rows,
    gate_w,
    up_w,
    down_w,
    hidden,
    gate_acc,
    up_acc,
    result,
    swap_send,
    swap_recv,
    back,
    w_sem,
    send_sem,
    recv_sem,
    h_send,
    h_recv,
    e_send,
    e_recv,
    b_send,
    b_recv,
):
    z, core, tp, sibling, x_peer, y_peer, chunks = place()
    chips, cap = out_going.shape[0], out_going.shape[1]
    part = cap // 2
    ahead = [{"sp": ((z + d) % chips) * 2 + core, "tp": tp} for d in range(chips)]
    behind = [{"sp": ((z + chips - d) % chips) * 2 + core, "tp": tp} for d in range(chips)]
    enter(ahead[1:] + [sibling, x_peer, y_peer])

    def slot(d, r, side=0):
        return rows.at[d, r, pl.ds(side * cap, cap)]

    Z, X, Y, VIA_X, VIA_Y, SIDE = 0, 1, 2, 3, 4, 5
    pending = []
    arrivals = {}

    def send(source, target, kind, d, device):
        copy = remote(source, target, send_sem.at[kind, d], recv_sem.at[kind, d], device)
        copy.start()
        pending.append(copy)
        arrivals[kind, d] = copy

    for d in range(1, chips):
        send(out_going.at[d], slot(d, 0), Z, d, ahead[d])
    loads = [
        pltpu.make_async_copy(source, target, w_sem.at[i])
        for i, (source, target) in enumerate(
            ((gate_hbm, gate_w), (up_hbm, up_w), (down_hbm, down_w))
        )
    ]

    def to_side(d, r):
        source = out_going.at[0] if d == 0 and r == 0 else slot(d, r)
        send(source, slot(d, r, 1), SIDE + r, d, sibling)

    def spread(d):
        source = out_going.at[0] if d == 0 else slot(d, 0)
        if d:
            arrivals[Z, d].wait_recv()
        send(source, slot(d, 1), X, d, x_peer)
        send(source, slot(d, 2), Y, d, y_peer)
        to_side(d, 0)

    def relay(d):
        for kind, r, peer in ((X, 1, y_peer), (Y, 2, x_peer)):
            arrivals[kind, d].wait_recv()
            piece = pl.ds((r - 1) * part, part)
            send(rows.at[d, r, piece], rows.at[d, 3, piece], VIA_X + r - 1, d, peer)
            to_side(d, r)

    def project(d):
        for r in range(4):
            if r == 3:
                arrivals[VIA_X, d].wait_recv()
                arrivals[VIA_Y, d].wait_recv()
                to_side(d, 3)
            arrivals[SIDE + r, d].wait_recv()
            block = rows[d, r, :, pl.ds(0, width)]
            for weight, total in ((gate_w, gate_acc), (up_w, up_acc)):
                product = jnp.dot(block, weight[chunks[r]], preferred_element_type=jnp.float32)
                if r == 0:
                    total[...] = product
                else:
                    total[...] += product
        squares = 0.0
        for r in range(4):
            extra = rows[d, r, :, pl.ds(width, EXTRA)].astype(jnp.float32)
            squares = squares + extra[:, 0:1] + extra[:, 1:2]
        scale = lax.rsqrt(squares / (4 * width) + epsilon)
        gate_value = gate_acc[...] * scale
        up_value = up_acc[...] * scale
        hidden[d, 0] = (gate_value / (1.0 + jnp.exp(-gate_value)) * up_value).astype(jnp.bfloat16)

    def send_hidden_piece(d, k, source, target, peer):
        copy = remote(source, target, h_send.at[d, k], h_recv.at[d, k], peer)
        copy.start()
        pending.append(copy)
        arrivals["h", d, k] = copy

    def spread_hidden(d):
        send_hidden_piece(d, 0, hidden.at[d, 0], hidden.at[d, 1], x_peer)
        send_hidden_piece(d, 1, hidden.at[d, 0], hidden.at[d, 2], y_peer)

    def relay_hidden(d):
        for k, peer in ((0, y_peer), (1, x_peer)):
            arrivals["h", d, k].wait_recv()
            piece = pl.ds(k * cap, cap)
            send_hidden_piece(d, 2 + k, hidden.at[d, 1 + k, piece], hidden.at[d, 3, piece], peer)

    def finish(d):
        for r in range(4):
            if r == 3:
                arrivals["h", d, 2].wait_recv()
                arrivals["h", d, 3].wait_recv()
            product = jnp.dot(hidden[d, r], down_w[chunks[r]], preferred_element_type=jnp.float32)
            if r == 0:
                result[...] = product
            else:
                result[...] += product
        extra = rows[d, 0, :, pl.ds(width, EXTRA)].astype(jnp.float32)
        low = extra[:, 2:3] + extra[:, 3:4]
        high = extra[:, 4:5] + extra[:, 5:6]
        share = low + (high - low) * core.astype(jnp.float32)
        swap_send[d] = (result[cap:, :] * share[cap:]).astype(jnp.bfloat16)
        copy = remote(swap_send.at[d], swap_recv.at[d], e_send.at[d], e_recv.at[d], sibling)
        copy.start()
        pending.append(copy)
        kept = result[:cap, :] * share[:cap]
        copy.wait_recv()
        total = (kept + swap_recv[d].astype(jnp.float32)).astype(jnp.bfloat16)
        if d == 0:
            out_ref[0] = total
            return
        back[d] = total
        copy = remote(back.at[d], out_ref.at[d], b_send.at[d], b_recv.at[d], behind[d])
        copy.start()
        pending.append(copy)
        arrivals["b", d] = copy

    spread(0)
    for copy in loads:
        copy.start()
    rows[0, 0, pl.ds(0, cap)] = out_going[0]
    relay(0)
    spread(1)
    relay(1)
    loads[0].wait()
    loads[1].wait()
    project(0)
    spread(2)
    project(1)
    spread_hidden(1)
    relay(2)
    spread(3)
    relay_hidden(1)
    project(2)
    spread_hidden(2)
    relay(3)
    loads[2].wait()
    finish(1)
    spread_hidden(0)
    relay_hidden(2)
    project(3)
    spread_hidden(3)
    finish(2)
    relay_hidden(0)
    relay_hidden(3)
    finish(3)
    finish(0)
    for d in range(1, chips):
        arrivals["b", d].wait_recv()
    for copy in pending:
        copy.wait_send()


def run_experts(out_going, gate_weight, up_weight, down_weight):
    chips, cap, padded = out_going.shape
    width, ff = (padded - EXTRA, gate_weight.shape[1])
    features = down_weight.shape[1]
    return pl.pallas_call(
        functools.partial(experts_kernel, width),
        out_shape=jax.ShapeDtypeStruct((chips, cap, features), jnp.bfloat16),
        in_specs=[pl.BlockSpec(memory_space=pltpu.VMEM)]
        + [pl.BlockSpec(memory_space=pl.ANY)] * 3,
        out_specs=pl.BlockSpec(memory_space=pltpu.VMEM),
        scratch_shapes=[
            pltpu.VMEM((chips, 4, 2 * cap, padded), jnp.bfloat16),
            pltpu.VMEM((4, width, ff), jnp.bfloat16),
            pltpu.VMEM((4, width, ff), jnp.bfloat16),
            pltpu.VMEM((4, ff, features), jnp.bfloat16),
            pltpu.VMEM((chips, 4, 2 * cap, ff), jnp.bfloat16),
            pltpu.VMEM((2 * cap, ff), jnp.float32),
            pltpu.VMEM((2 * cap, ff), jnp.float32),
            pltpu.VMEM((2 * cap, features), jnp.float32),
            pltpu.VMEM((chips, cap, features), jnp.bfloat16),
            pltpu.VMEM((chips, cap, features), jnp.bfloat16),
            pltpu.VMEM((chips, cap, features), jnp.bfloat16),
            pltpu.SemaphoreType.DMA((3,)),
            pltpu.SemaphoreType.DMA((9, chips)),
            pltpu.SemaphoreType.DMA((9, chips)),
            pltpu.SemaphoreType.DMA((chips, 4)),
            pltpu.SemaphoreType.DMA((chips, 4)),
            pltpu.SemaphoreType.DMA((chips,)),
            pltpu.SemaphoreType.DMA((chips,)),
            pltpu.SemaphoreType.DMA((chips,)),
            pltpu.SemaphoreType.DMA((chips,)),
        ],
        compiler_params=pltpu.CompilerParams(
            collective_id=2, has_side_effects=True, vmem_limit_bytes=56 * 1024 * 1024
        ),
    )(
        out_going,
        gate_weight.reshape(4, width, ff),
        up_weight.reshape(4, width, ff),
        down_weight.reshape(4, ff, features),
    )


def split_pair(values):
    high = lax.reduce_precision(values, 8, 7)
    return high, values - high


def paired_block(
    chips,
    positions,
    tokens,
    lean,
    lean_gains,
    broad,
    broad_gains,
    mixer_gain,
    output_weight,
    channel_gain,
    expert_weights,
    route_experts,
    weights,
):
    row_count, width = tokens.shape
    cap = row_count // 2
    group = route_experts[:, 0] // 2
    near = (group + GROUPS - lax.axis_index("sp") // 2) % GROUPS
    member = (near[:, None] == jnp.arange(GROUPS, dtype=jnp.int32)[None, :]).astype(jnp.bfloat16)
    order = jnp.arange(row_count, dtype=jnp.int32)
    earlier = (order[:, None] > order[None, :]).astype(jnp.bfloat16)
    counts = jnp.dot(earlier, member, preferred_element_type=jnp.float32)
    rank = jnp.sum(counts * member.astype(jnp.float32), axis=1).astype(jnp.int32)
    slot_index = near * cap + rank
    slots = jnp.arange(GROUPS * cap, dtype=jnp.int32)
    picker = (slots[:, None] == slot_index[None, :]).astype(jnp.bfloat16)
    first_low = route_experts[:, 0] % 2 == 0
    low = jnp.where(first_low, weights[:, 0], weights[:, 1])
    high = jnp.where(first_low, weights[:, 1], weights[:, 0])
    lane = jnp.arange(EXTRA, dtype=jnp.int32)[None, :]
    route_columns = jnp.zeros((row_count, EXTRA), jnp.float32)
    for i, column in enumerate(split_pair(low) + split_pair(high)):
        route_columns = jnp.where(lane == 2 + i, column[:, None], route_columns)
    stream, out_going = run_front(
        chips,
        positions,
        lean,
        broad,
        lean_gains,
        broad_gains,
        mixer_gain,
        tokens,
        channel_gain,
        picker,
        route_columns,
        output_weight,
    )
    arrived = run_experts(out_going.reshape(GROUPS, cap, width + EXTRA), *expert_weights)
    arrived = arrived.reshape(GROUPS * cap, width)
    picked = lax.dot_general(
        picker, arrived, (((0,), (0,)), ((), ())), preferred_element_type=jnp.float32
    )
    return (stream + picked).astype(jnp.bfloat16)


def on_device(
    tokens,
    lean_query,
    lean_key,
    lean_value,
    lean_gains,
    broad_query,
    broad_key,
    broad_value,
    broad_gains,
    mixer_gain,
    output_weight,
    channel_gain,
    gate_weight,
    up_weight,
    down_weight,
    route_experts,
    route_logits,
    group_weight,
):
    row_count = tokens.shape[0]
    positions = lax.axis_index("sp") * row_count + jnp.arange(row_count, dtype=jnp.int32)
    lane_index = lax.axis_index("tp")
    logit_gap = route_logits[:, 0] - route_logits[:, 1]
    weights = group_weight[:, None] * jax.nn.sigmoid(jnp.stack([logit_gap, -logit_gap], axis=1))
    chips = lax.axis_size("sp") // 2
    if (
        lax.axis_size("tp") == 4
        and chips == GROUPS
        and chips == 4
        and route_experts.shape[1] == 2
        and lean_query.shape[1:] == (4, 64)
        and broad_query.shape[1:] == (4, 128)
        and lean_key.shape[1:] == (2, 64)
        and broad_key.shape[1:] == (2, 128)
    ):
        return paired_block(
            chips,
            positions,
            tokens,
            (lean_query, lean_key, lean_value),
            lean_gains,
            (broad_query, broad_key, broad_value),
            broad_gains,
            mixer_gain,
            output_weight,
            channel_gain,
            (gate_weight[0], up_weight[0], down_weight[0]),
            route_experts,
            weights,
        )
    lean_queries, lean_keys, lean_values = own_heads(
        lean_query, lean_key, lean_value, lean_gains, positions, lane_index, HQ_A // KV_A
    )
    broad_queries, broad_keys, broad_values = own_heads(
        broad_query, broad_key, broad_value, broad_gains, positions, lane_index, HQ_B // KV_B
    )
    shard_rows = (
        lax.all_gather(lean_keys, "sp", axis=0, tiled=True),
        lax.all_gather(lean_values, "sp", axis=0, tiled=True),
        lax.all_gather(broad_keys, "sp", axis=0, tiled=True),
        lax.all_gather(broad_values, "sp", axis=0, tiled=True),
    )
    lean_state = attend_piece(start_state(lean_queries), lean_queries, shard_rows[0], shard_rows[1])
    broad_state = attend_piece(
        start_state(broad_queries), broad_queries, shard_rows[2], shard_rows[3]
    )
    lean_all, broad_all = (
        lax.all_gather(finish_heads(lean_state), "tp", axis=1, tiled=True),
        lax.all_gather(finish_heads(broad_state), "tp", axis=1, tiled=True),
    )
    lean_width = lean_all.shape[1]
    stream = tokens.astype(jnp.float32) + jnp.dot(
        group_norm(lean_all, mixer_gain[:lean_width]),
        output_weight[:lean_width],
        preferred_element_type=jnp.float32,
    )
    stream = stream + jnp.dot(
        group_norm(broad_all, mixer_gain[lean_width:]),
        output_weight[lean_width:],
        preferred_element_type=jnp.float32,
    )
    squares = lax.psum(jnp.sum(stream * stream, axis=1), "tp")
    normed = (stream * lax.rsqrt(squares / D + epsilon)[:, None] * channel_gain).astype(
        jnp.bfloat16
    )
    experts = lax.axis_size("sp")
    capacity = row_count // (experts // GROUPS)
    flat_experts = route_experts.reshape(-1)
    onehot = (flat_experts[:, None] == jnp.arange(experts, dtype=jnp.int32)[None, :]).astype(
        jnp.int32
    )
    slot_rank = jnp.sum((jnp.cumsum(onehot, axis=0) - 1) * onehot, axis=1)
    slot_index = flat_experts * capacity + slot_rank
    token_owner = jnp.repeat(jnp.arange(row_count, dtype=jnp.int32), route_experts.shape[1])
    filled = jnp.zeros((experts * capacity,), jnp.int32).at[slot_index].set(token_owner + 1)
    slot_live = (filled > 0)[:, None]
    source = jnp.maximum(filled - 1, 0)
    outgoing = jnp.where(slot_live, normed[source], jnp.zeros((), jnp.bfloat16)).reshape(
        experts, capacity, -1
    )
    arrived = lax.all_to_all(outgoing, "sp", split_axis=0, concat_axis=0, tiled=True)
    sources = arrived.shape[0]
    item_count = arrived.shape[1]
    shard_rows = lax.all_gather(arrived, "tp", axis=2, tiled=True)
    flat_rows = shard_rows.reshape(sources * item_count, shard_rows.shape[2])
    gate_part = gate_weight[0]
    up_part = up_weight[0]
    gate_value = jnp.dot(flat_rows, gate_part, preferred_element_type=jnp.float32)
    up_value = jnp.dot(flat_rows, up_part, preferred_element_type=jnp.float32)
    hidden = (jax.nn.silu(gate_value) * up_value).astype(jnp.bfloat16)
    down_part = down_weight[0]
    result = jnp.dot(
        lax.all_gather(hidden, "tp", axis=1, tiled=True),
        down_part,
        preferred_element_type=jnp.float32,
    )
    result = result.astype(jnp.bfloat16).reshape(sources, item_count, -1)
    returned = lax.all_to_all(result, "sp", split_axis=0, concat_axis=0, tiled=True)
    picked = (
        returned.reshape(experts * capacity, -1)[slot_index]
        .reshape(row_count, route_experts.shape[1], -1)
        .astype(jnp.float32)
    )
    return (stream + jnp.sum(picked * weights[:, :, None], axis=1)).astype(jnp.bfloat16)


def solution(mesh):
    return jax.shard_map(
        on_device,
        mesh=mesh,
        in_specs=(
            P("sp", "tp"),
            P("sp", "tp", None),
            P("sp", None, None),
            P("sp", None, None),
            P(),
            P("sp", "tp", None),
            P("sp", None, None),
            P("sp", None, None),
            P(),
            P(),
            P(None, "tp"),
            P("tp"),
            P("sp", None, "tp"),
            P("sp", None, "tp"),
            P("sp", None, "tp"),
            P("sp", None),
            P("sp", None),
            P("sp"),
        ),
        out_specs=P("sp", "tp"),
        check_vma=False,
    )
```

profile of v0, /device:TPU:0, one launch (start us, length us, event | category | flops | bytes accessed | tf_op | source)
XLA Modules:
  0.0 134.1 jit_solution(15191897915338832988)
XLA Ops:
  0.0 0.8 pad_maximum_fusion.lean_gain
  0.9 0.8 fusion.18
  1.6 0.7 fusion.9
  2.3 0.7 reduce-precision_subtract_fusion.1
  3.1 0.7 fusion.19
  3.8 0.2 fusion.1
  4.0 0.9 copy.26.lean_k
  4.9 1.0 copy.27.lean_v
  5.9 0.2 select_select_fusion.route_columns
  6.1 1.0 copy.25.lean_q
  7.1 1.0 copy.34
  8.1 1.0 copy_bitcast_fusion.1
  9.1 1.5 %sine_multiply_fusion = (f32[192,256]{1,0:T(8,128)S(1)}, f32[192,256]{1,0:T(8,128)S(1)}) fusion(f32[256]{0:T(256)} %constant.104, f32[256]{0:T(256)} %constant.103, f32[192]{0:T(256)S(1)} %get-tuple-element.20, f32[192]{0:T(256)S(1)} %get-tuple-element.21, pred[256]{0:T(512)(128)(4,1)} %constant.102), kind=kLoop, calls=%fused_computation.9 | loop fusion | flops 147456 | bytes 397056 | tf_op jit(solution)/shard_map/mul | solution.py:476
  10.5 0.0 copy-start.1
  10.6 1.0 copy-done.1
  11.5 0.0 copy-start.2
  11.5 0.7 copy-done.2
  12.3 0.0 copy-start.3
  12.3 0.7 copy-done.3
  12.9 0.0 copy-start.4
  12.9 0.7 copy-done.4
  13.6 43.0 %shard_map.199 = (f32[192,1024]{1,0:T(8,128)S(1)}, bf16[384,1152]{1,0:T(8,128)(2,1)S(1)}) custom-call(bf16[192,256]{1,0:T(8,128)(2,1)S(1)} %copy.25.lean_q, bf16[192,128]{1,0:T(8,128)(2,1)S(1)} %copy.26.lean_k, bf16[192,128]{1,0:T(8,128)(2,1)S(1)} %copy.27.lean_v, bf16[192,512]{1,0:T(8,128)(2,1)S(1)} %bitcast.28, ...), custom_call_target="tpu_custom_call" | custom-call | tf_op jit(solution)/shard_map/pallas_call | solution.py:441
  56.6 0.0 copy-start
  56.7 0.9 copy-done
  57.6 74.2 %shard_map.200 = bf16[4,96,1024]{2,1,0:T(8,128)(2,1)} custom-call(bf16[4,96,1152]{2,1,0:T(8,128)(2,1)} %bitcast.27, bf16[4,1024,512]{2,1,0:T(8,128)(2,1)} %bitcast.31, bf16[4,1024,512]{2,1,0:T(8,128)(2,1)} %bitcast.32, bf16[4,512,1024]{2,1,0:T(8,128)(2,1)} %bitcast.33), custom_call_target="tpu_custom_call" | custom-call | tf_op jit(solution)/shard_map/pallas_call | solution.py:671
  131.8 2.3 %fusion = bf16[192,1024]{1,0:T(8,128)(2,1)} fusion(f32[192,1024]{1,0:T(8,128)S(1)} %get-tuple-element.7, bf16[384,1024]{1,0:T(8,128)(2,1)} %bitcast.34, s32[192]{0:T(256)S(1)} %fusion.13), kind=kOutput, calls=%fused_computation.1 | convolution fusion | flops 151461888 | bytes 1966848 | tf_op jit(solution)/shard_map/dot_general | solution.py:765
  (8 shorter events, 0.1 us)
Async XLA Ops:
  10.5 1.0 copy-start.1
  11.5 0.7 copy-start.2
  12.3 0.7 copy-start.3
  12.9 0.7 copy-start.4
  56.6 0.9 copy-start
where the time goes:
time: 136 us; the launch traced here: 134 us
  Pallas kernels  117 us (86%)
  local copies, waits for them, and re-layouts  8.8 us (6%)
  other arithmetic  5.46 us (4%)
  matrix products  2.47 us (2%)
    pallas_call x1, Pallas kernels, run_experts(): pl.pallas_call(functools.partial(experts_kernel, width), out_shape=jax.Sh...  74.2 us
    pallas_call x1, Pallas kernels, run_front(): pl.pallas_call(functools.partial(front_kernel, chips), out_shape=[jax.Sha...  43 us
    unnamed x11, local copies, waits for them, and re-layouts  4.93 us
    reshape x4, local copies, waits for them, and re-layouts, run_front(): flat = [part.reshape(rows, -1) for part in lean + broad]  3.87 us

commit v1 on v0

v1 whole, which is shorter than its diff:
```python
import functools

import jax
import jax.numpy as jnp
import numpy as np
from jax import lax
from jax.experimental import pallas as pl
from jax.experimental.pallas import tpu as pltpu
from jax.sharding import PartitionSpec as P

D = 4096
HQ_A = 16
KV_A = 2
HQ_B = 16
KV_B = 2
GRID_W = 64
GROUPS = 4


epsilon = 1e-06
theta_base = 10000.0
floor_score = -1e30


def axial_angles(positions, head_size):
    quarter = head_size // 4
    frequency = theta_base ** (-jnp.arange(quarter, dtype=jnp.float32) / quarter)
    grid_rows = (positions // GRID_W).astype(jnp.float32)
    grid_columns = (positions % GRID_W).astype(jnp.float32)
    return (grid_rows[:, None] * frequency[None, :], grid_columns[:, None] * frequency[None, :])


def turn_half(values, angles):
    half_width = values.shape[-1] // 2
    first_half = values[..., :half_width]
    second = values[..., half_width:]
    cosine = jnp.cos(angles)[:, None, :]
    sine_part = jnp.sin(angles)[:, None, :]
    return jnp.concatenate(
        [first_half * cosine - second * sine_part, second * cosine + first_half * sine_part],
        axis=-1,
    )


def prepare(raw_values, gain_row, positions):
    values = raw_values.astype(jnp.float32)
    values = (
        values * lax.rsqrt(jnp.mean(values * values, axis=-1, keepdims=True) + epsilon) * gain_row
    )
    row_angles, column_angles = axial_angles(positions, raw_values.shape[-1])
    half_width = raw_values.shape[-1] // 2
    turned = jnp.concatenate(
        [
            turn_half(values[..., :half_width], row_angles),
            turn_half(values[..., half_width:], column_angles),
        ],
        axis=-1,
    )
    return turned.astype(jnp.bfloat16)


def group_norm(head_rows, gain_row):
    values = head_rows.astype(jnp.float32)
    return (
        values * lax.rsqrt(jnp.mean(values * values, axis=-1, keepdims=True) + epsilon) * gain_row
    ).astype(jnp.bfloat16)


def own_heads(query_raw, key_raw, value_raw, gain_pair, positions, lane_index, group_ratio):
    head_count, head_size = (query_raw.shape[1], query_raw.shape[2])
    key_heads = max(1, head_count // group_ratio)
    kv_start = lane_index * head_count // group_ratio
    key_part = lax.dynamic_slice_in_dim(key_raw, kv_start, key_heads, 1)
    value_part = lax.dynamic_slice_in_dim(value_raw, kv_start, key_heads, 1)
    queries = prepare(query_raw, gain_pair[0], positions).reshape(
        query_raw.shape[0], key_heads, head_count // key_heads, head_size
    )
    return (queries, prepare(key_part, gain_pair[1], positions), value_part)


def start_state(queries):
    row_count = queries.shape[0]
    head_count = queries.shape[1] * queries.shape[2]
    return (
        jnp.full((head_count, row_count), floor_score, jnp.float32),
        jnp.zeros((head_count, row_count), jnp.float32),
        jnp.zeros((row_count, head_count, queries.shape[3]), jnp.float32),
    )


def attend_piece(fold_state, queries, keys, values):
    peak_score, weight_sum, accumulated = fold_state
    row_count, key_heads, grouped, head_size = queries.shape
    key_count = keys.shape[0]
    scores = jnp.einsum(
        "qkgd,skd->kgqs", queries, keys, preferred_element_type=jnp.float32
    ) * head_size ** (-0.5)
    scores = scores.reshape(key_heads * grouped, row_count, key_count)
    new_peak = jnp.maximum(peak_score, jnp.max(scores, axis=-1))
    weights = jnp.exp(scores - new_peak[..., None])
    new_sum = jnp.sum(weights, axis=-1)
    rounded = weights.astype(jnp.bfloat16).reshape(key_heads, grouped, row_count, key_count)
    partial_value = jnp.einsum(
        "kgqs,skd->qkgd", rounded, values, preferred_element_type=jnp.float32
    )
    partial_value = partial_value.reshape(row_count, key_heads * grouped, head_size)
    return (new_peak, new_sum, partial_value)


def finish_heads(fold_state):
    accumulated = fold_state[2]
    return (
        (accumulated / jnp.transpose(fold_state[1])[:, :, None])
        .astype(jnp.bfloat16)
        .reshape(accumulated.shape[0], -1)
    )


MESH = pl.DeviceIdType.MESH
COPIES = 160
LOG2E = 1.4426950408889634


def remote(source, target, send_sem, recv_sem, device):
    return pltpu.make_async_remote_copy(
        src_ref=source,
        dst_ref=target,
        send_sem=send_sem,
        recv_sem=recv_sem,
        device_id=device,
        device_id_type=MESH,
    )


def eye(size, dtype):
    rows = lax.broadcasted_iota(jnp.int32, (size, size), 0)
    columns = lax.broadcasted_iota(jnp.int32, (size, size), 1)
    return jnp.where(rows == columns, 1.0, 0.0).astype(dtype)


def to_column(row):
    size = row.shape[1]
    rows = lax.broadcasted_iota(jnp.int32, (size, size), 0)
    columns = lax.broadcasted_iota(jnp.int32, (size, size), 1)
    spread = jnp.broadcast_to(row, (size, size))
    return jnp.sum(jnp.where(rows == columns, spread, 0.0), axis=1, keepdims=True)


def to_row(column):
    size = column.shape[0]
    rows = lax.broadcasted_iota(jnp.int32, (size, size), 0)
    columns = lax.broadcasted_iota(jnp.int32, (size, size), 1)
    spread = jnp.broadcast_to(column, (size, size))
    return jnp.sum(jnp.where(rows == columns, spread, 0.0), axis=0, keepdims=True)


def dot_nt(left, right):
    return lax.dot_general(
        left, right, (((1,), (1,)), ((), ())), preferred_element_type=jnp.float32
    )


def layer_kernel(
    chips,
    lean_q_hbm,
    lean_k_hbm,
    lean_v_hbm,
    broad_q_hbm,
    broad_k_hbm,
    broad_v_hbm,
    lean_gain_hbm,
    broad_gain_hbm,
    lean_rows_hbm,
    lean_columns_hbm,
    broad_rows_hbm,
    broad_columns_hbm,
    experts_hbm,
    logits_hbm,
    group_hbm,
    mixer_hbm,
    tokens_hbm,
    channel_hbm,
    weight_hbm,
    gate_hbm,
    up_hbm,
    down_hbm,
    out_ref,
    lean_q,
    lean_k,
    lean_v,
    broad_q,
    broad_k,
    broad_v,
    lean_gain,
    broad_gain,
    lean_rows,
    lean_columns,
    broad_rows,
    broad_columns,
    experts,
    logits,
    group_weight,
    mixer_gain,
    tokens,
    channel_gain,
    weight,
    gate_w,
    up_w,
    down_w,
    pairs_f32,
    own,
    keys,
    queries,
    peak,
    total,
    lean_mass,
    broad_mass,
    lean_heads,
    broad_heads,
    lean_acc,
    broad_acc,
    stream,
    scaled,
    picker,
    unpicker,
    routes,
    norms,
    extras,
    going,
    rows,
    gate_acc,
    up_acc,
    hidden,
    result,
    swap_send,
    swap_recv,
    back,
    arrived,
    load_sem,
    send_sem,
    recv_sem,
):
    sp, tp = lax.axis_index("sp"), lax.axis_index("tp")
    z, core = sp // 2, sp % 2
    y, x = tp // 2, tp % 2
    sibling = {"sp": z * 2 + (1 - core), "tp": tp}
    x_peer = {"sp": sp, "tp": y * 2 + (1 - x)}
    y_peer = {"sp": sp, "tp": (1 - y) * 2 + x}
    far_peer = {"sp": sp, "tp": (1 - y) * 2 + (1 - x)}
    chunks = (tp, y * 2 + (1 - x), (1 - y) * 2 + x, (1 - y) * 2 + (1 - x))
    ahead = [{"sp": ((z + d) % chips) * 2 + core, "tp": tp} for d in range(chips)]
    behind = [{"sp": ((z + chips - d) % chips) * 2 + core, "tp": tp} for d in range(chips)]
    peers = ahead[1:] + [sibling, x_peer, y_peer, far_peer]
    barrier = pltpu.get_barrier_semaphore()
    for peer in peers:
        pl.semaphore_signal(barrier, inc=1, device_id=peer, device_id_type=MESH)

    count = own.shape[0]
    half = count // 2
    cap = count // 2
    lanes = 128
    width = tokens.shape[1]
    heads = lean_q.shape[0]
    tile = count
    tiles = heads

    loads = []

    def load(source, target):
        copy = pltpu.make_async_copy(source, target, load_sem.at[len(loads)])
        copy.start()
        loads.append(copy)
        return copy

    first_loads = [
        load(broad_k_hbm, broad_k),
        load(broad_v_hbm, broad_v),
        load(lean_k_hbm, lean_k),
        load(lean_v_hbm, lean_v),
        load(lean_gain_hbm, lean_gain),
        load(broad_gain_hbm, broad_gain),
        load(lean_rows_hbm.at[sp], lean_rows),
        load(lean_columns_hbm, lean_columns),
        load(broad_rows_hbm.at[sp], broad_rows),
        load(broad_columns_hbm, broad_columns),
    ]
    query_loads = [load(broad_q_hbm, broad_q), load(lean_q_hbm, lean_q)]
    route_loads = [
        load(experts_hbm, experts),
        load(logits_hbm, logits),
        load(group_hbm, group_weight),
        load(mixer_hbm, mixer_gain),
        load(tokens_hbm, tokens),
        load(channel_hbm, channel_gain),
    ]
    weight_load = load(weight_hbm, weight)
    gate_loads = [load(gate_hbm, gate_w), load(up_hbm, up_w)]
    down_load = load(down_hbm, down_w)

    pending = []
    arrivals = {}

    def send(key, source, target, device):
        n = len(pending)
        copy = remote(source, target, send_sem.at[n], recv_sem.at[n], device)
        copy.start()
        pending.append(copy)
        arrivals[key] = copy

    def arrive(*key):
        arrivals[key].wait_recv()

    unit = eye(count, jnp.bfloat16)

    def broad_turned(raw, gain, columns, row_values):
        values = raw.astype(jnp.float32)
        mean = jnp.sum(values * values, axis=1, keepdims=True) / lanes
        values = values * lax.rsqrt(mean + epsilon) * gain
        quarter = lanes // 4
        lane = lax.broadcasted_iota(jnp.int32, values.shape, 1)
        partner = jnp.where(
            lane % (2 * quarter) < quarter,
            pltpu.roll(values, lanes - quarter, 1),
            pltpu.roll(values, quarter, 1),
        )
        cosine = columns[0] + row_values[:, :lanes]
        sine = columns[1] + row_values[:, lanes:]
        return values * cosine + partner * sine

    def lean_turned(raw, gain):
        values = raw.astype(jnp.float32)
        size = values.shape[0]
        quarter = size // 4
        mean = jnp.sum(values * values, axis=0, keepdims=True) / size
        values = values * lax.rsqrt(mean + epsilon) * gain
        turned = []
        for start, table in ((0, lean_rows), (size // 2, lean_columns)):
            u = values[start : start + quarter]
            w = values[start + quarter : start + 2 * quarter]
            cosine, sine = table[:quarter], table[quarter:]
            turned += [u * cosine - w * sine, w * cosine + u * sine]
        return jnp.concatenate(turned, axis=0)

    for copy in first_loads:
        copy.wait()
    key_heads = lean_k.shape[0]
    pairs_f32[0] = broad_k[...].astype(jnp.float32)
    pairs_f32[1] = broad_v[...].astype(jnp.float32)
    grid_rows = broad_rows.shape[0]
    run = count // grid_rows
    for i in range(grid_rows):
        part = pl.ds(i * run, run)
        picked = pl.ds(y + i * run * key_heads, run, stride=key_heads)
        columns = [broad_columns[k, pl.ds(0, run, stride=heads), :] for k in range(2)]
        own[part, :lanes] = broad_turned(
            pairs_f32[0, picked, :], broad_gain[1:2, :], columns, broad_rows[i : i + 1, :]
        ).astype(jnp.bfloat16)
        own[part, lanes : 2 * lanes] = pairs_f32[1, picked, :].astype(jnp.bfloat16)
    size = lean_k.shape[1]
    lean_pair = jnp.concatenate(
        [lean_turned(lean_k[y], to_column(lean_gain[1:2, :])).astype(jnp.bfloat16), lean_v[y]],
        axis=0,
    )
    own[:, 2 * lanes :] = dot_nt(unit, lean_pair).astype(jnp.bfloat16)

    pl.semaphore_wait(barrier, len(peers))
    mine = pl.ds(pl.multiple_of(x * half, half), half)
    other = pl.ds(pl.multiple_of((1 - x) * half, half), half)
    side_mine = pl.ds(pl.multiple_of(count + x * half, half), half)
    side_other = pl.ds(pl.multiple_of(count + (1 - x) * half, half), half)
    for d in range(1, chips):
        send(("kz", d), own.at[mine], keys.at[d, mine], ahead[d])
    send(("ka", 0), own, keys.at[0, pl.ds(count, count)], sibling)
    keys[0, pl.ds(0, count)] = own[...]

    for copy in query_loads:
        copy.wait()
    q_run = run * heads
    for i in range(grid_rows):
        part = pl.ds(i * q_run, q_run)
        queries[1, part] = broad_turned(
            broad_q[part, :], broad_gain[0:1, :], broad_columns, broad_rows[i : i + 1, :]
        ).astype(jnp.bfloat16)
    query_gain = to_column(lean_gain[0:1, :])
    blank = jnp.zeros((lanes - size, count), jnp.bfloat16)
    for h in range(heads):
        turned = lean_turned(lean_q[h], query_gain).astype(jnp.bfloat16)
        queries[0, pl.ds(h * count, count)] = dot_nt(
            unit, jnp.concatenate([turned, blank], axis=0)
        ).astype(jnp.bfloat16)

    def attend(d, kind, start, stop):
        head_size = size if kind == 0 else lanes
        scale = head_size ** (-0.5) * LOG2E
        key_part = pl.ds(2 * lanes, lanes) if kind == 0 else pl.ds(0, lanes)
        value_part = pl.ds(2 * lanes, lanes) if kind == 0 else pl.ds(lanes, lanes)
        mass = lean_mass if kind == 0 else broad_mass

        def one_tile(i):
            part = pl.ds(pl.multiple_of(i * tile, tile), tile)
            scores = dot_nt(queries[kind, part], keys[d, :, key_part])
            top = jnp.max(scores, axis=1, keepdims=True)
            if d:
                old = peak[kind, part][:, :1]
                top = jnp.maximum(old, top)
            weights = jnp.exp2((scores - top) * scale)
            summed = jnp.sum(weights, axis=1, keepdims=True)
            partial = jnp.dot(
                weights.astype(jnp.bfloat16),
                keys[d, :, value_part],
                preferred_element_type=jnp.float32,
            )
            if d:
                shrink = jnp.exp2((old - top) * scale)
                summed = summed + total[kind, part][:, :1] * shrink
                partial = partial + mass[part] * shrink
            if d + 1 < chips:
                peak[kind, part] = jnp.broadcast_to(top, (tile, lanes))
                total[kind, part] = jnp.broadcast_to(summed, (tile, lanes))
                mass[part] = partial
            else:
                mass[part] = partial / summed

        def two_tiles(i, carry):
            one_tile(2 * i)
            one_tile(2 * i + 1)
            return carry

        lax.fori_loop(start // 2, stop // 2, two_tiles, 0)

    def forward(d):
        arrive("kz", d)
        send(("kx", d), keys.at[d, mine], keys.at[d, mine], x_peer)
        send(("ka", d), keys.at[d, mine], keys.at[d, side_mine], sibling)

    def forward_other(d):
        arrive("kx", d)
        send(("kb", d), keys.at[d, other], keys.at[d, side_other], sibling)

    for copy in route_loads:
        copy.wait()
    group = experts[0:1, :] // 2
    near = (group + chips - z) % chips
    first_low = experts[0:1, :] % 2 == 0
    gap = logits[0:1, :] - logits[1:2, :]
    first_weight = group_weight[...] / (1.0 + jnp.exp(-gap))
    second_weight = group_weight[...] / (1.0 + jnp.exp(gap))
    low_weight = jnp.where(first_low, first_weight, second_weight)
    high_weight = jnp.where(first_low, second_weight, first_weight)
    line = lax.broadcasted_iota(jnp.int32, (8, count), 0)
    routes[...] = jnp.where(line == 1, low_weight, jnp.where(line == 2, high_weight, 0.0))
    member = jnp.where(line == near, 1.0, 0.0).astype(jnp.bfloat16)
    square_rows = lax.broadcasted_iota(jnp.int32, (count, count), 0)
    square_columns = lax.broadcasted_iota(jnp.int32, (count, count), 1)
    earlier = jnp.where(square_rows < square_columns, 1.0, 0.0).astype(jnp.bfloat16)
    ranks = jnp.dot(member, earlier, preferred_element_type=jnp.float32)
    slot = lax.broadcasted_iota(jnp.int32, (cap, count), 0).astype(jnp.float32)
    for d in range(chips):
        rank = jnp.where(near == d, ranks[d : d + 1, :], -1.0)
        picker[pl.ds(d * cap, cap), :] = jnp.where(slot == rank, 1.0, 0.0).astype(jnp.bfloat16)
    unpicker[...] = dot_nt(unit, picker[...]).astype(jnp.bfloat16)

    arrive("ka", 0)
    attend(0, 0, 0, tiles)
    forward(1)
    attend(0, 1, 0, tiles)
    forward_other(1)
    for d in range(1, chips - 1):
        forward(d + 1)
        arrive("ka", d)
        arrive("kb", d)
        attend(d, 0, 0, tiles)
        forward_other(d + 1)
        attend(d, 1, 0, tiles)

    piece_rows = half
    relay_rows = piece_rows // 2

    def spread_heads(kind, p):
        buffer = (lean_heads, broad_heads)[kind]
        part = pl.ds(p * piece_rows, piece_rows)
        for k, peer in ((0, x_peer), (1, y_peer)):
            send(("h", kind, p, k), buffer.at[0, part], buffer.at[1 + k, part], peer)

    def relay_heads(kind, p):
        buffer = (lean_heads, broad_heads)[kind]
        for k, peer in ((0, y_peer), (1, x_peer)):
            arrive("h", kind, p, k)
            part = pl.ds(p * piece_rows + k * relay_rows, relay_rows)
            send(("h", kind, p, 2 + k), buffer.at[1 + k, part], buffer.at[3, part], peer)

    lean_low = lax.broadcasted_iota(jnp.int32, (count, lanes), 1) < lanes // 2
    last = chips - 1
    arrive("ka", last)
    arrive("kb", last)
    attend(last, 0, 0, tiles)
    for h in range(heads // 2):
        first = lean_mass[pl.ds(2 * h * count, count), :]
        second = lean_mass[pl.ds((2 * h + 1) * count, count), :]
        pair = jnp.where(lean_low, pltpu.roll(first, lanes // 2, 1), second)
        lean_heads[0, :, pl.ds(h * lanes, lanes)] = pair.astype(jnp.bfloat16)
    spread_heads(0, 0)
    spread_heads(0, 1)
    for p in range(2):
        attend(last, 1, p * tiles // 2, (p + 1) * tiles // 2)
        for h in range(heads):
            picked = pl.ds(p * piece_rows * heads + h, piece_rows, stride=heads)
            broad_heads[0, pl.ds(p * piece_rows, piece_rows), pl.ds(h * lanes, lanes)] = broad_mass[
                picked, :
            ].astype(jnp.bfloat16)
        spread_heads(1, p)
        relay_heads(0, p)
    weight_load.wait()
    lean_width, broad_width = lean_heads.shape[2], broad_heads.shape[2]
    squares = [0.0, 0.0]

    def mix(kind, r):
        buffer, acc, span, start = (
            (lean_heads, lean_acc, lean_width, 0),
            (broad_heads, broad_acc, broad_width, 4 * lean_width),
        )[kind]
        part = pl.ds(pl.multiple_of(start + chunks[r] * span, span), span)
        values = buffer[r].astype(jnp.float32)
        squares[kind] = squares[kind] + jnp.sum(values * values, axis=1, keepdims=True)
        gained = (values * mixer_gain[:, part]).astype(jnp.bfloat16)
        product = jnp.dot(gained, weight[part, :], preferred_element_type=jnp.float32)
        if r == 0:
            acc[...] = product
        else:
            acc[...] += product

    mix(0, 0)
    mix(1, 0)
    relay_heads(1, 0)
    mix(0, 1)
    mix(0, 2)
    relay_heads(1, 1)
    for p in range(2):
        arrive("h", 0, p, 2)
        arrive("h", 0, p, 3)
    mix(0, 3)
    mix(1, 1)
    mix(1, 2)
    for p in range(2):
        arrive("h", 1, p, 2)
        arrive("h", 1, p, 3)
    mix(1, 3)
    lean_scale = lax.rsqrt(squares[0] / (4 * lean_width) + epsilon)
    broad_scale = lax.rsqrt(squares[1] / (4 * broad_width) + epsilon)
    values = (
        tokens[...].astype(jnp.float32)
        + lean_acc[...] * lean_scale
        + broad_acc[...] * broad_scale
    )
    stream[...] = values
    scaled[...] = (values * channel_gain[...]).astype(jnp.bfloat16)
    norm = to_row(jnp.sum(values * values, axis=1, keepdims=True))
    norms[0] = jnp.broadcast_to(norm, (8, count))
    for r, peer in ((1, x_peer), (2, y_peer), (3, far_peer)):
        send(("norm", r), norms.at[0], norms.at[r], peer)

    def pick(d):
        return jnp.dot(
            picker[pl.ds(d * cap, cap), :], scaled[...], preferred_element_type=jnp.float32
        ).astype(jnp.bfloat16)

    piece = cap // 2

    def slot_rows(d, r, side=0):
        return rows.at[d, r, pl.ds(side * cap, cap)]

    def spread(d):
        if d:
            arrive("z", d)
        for k in range(2):
            part, rest = pl.ds(k * piece, piece), pl.ds((1 - k) * piece, piece)
            send(("x", d, k), rows.at[d, 0, part], rows.at[d, 1, part], x_peer)
            send(("y", d, k), rows.at[d, 0, rest], rows.at[d, 2, rest], y_peer)
        send(("side", d, 0), slot_rows(d, 0), slot_rows(d, 0, 1), sibling)

    def relay(d):
        for k, axis, peer in ((0, "x", y_peer), (1, "y", x_peer)):
            arrive(axis, d, 0)
            part = pl.ds(k * piece, piece)
            send(("via", d, k), rows.at[d, 1 + k, part], rows.at[d, 3, part], peer)

    def sides(d):
        for r, axis in ((1, "x"), (2, "y")):
            arrive(axis, d, 1)
            send(("side", d, r), slot_rows(d, r), slot_rows(d, r, 1), sibling)

    def last_side(d):
        arrive("via", d, 0)
        arrive("via", d, 1)
        send(("side", d, 3), slot_rows(d, 3), slot_rows(d, 3, 1), sibling)

    def extra_side(d):
        if d:
            arrive("ez", d)
        send(("es", d), extras.at[0, d], extras.at[1, d], sibling)

    def extra_columns(d, line):
        return jnp.concatenate(
            [to_column(extras[side, d][line : line + 1, :])[:cap] for side in range(2)], axis=0
        )

    def project(d):
        last_side(d)
        for r in range(4):
            arrive("side", d, r)
            block = rows[d, r]
            for source, acc in ((gate_w, gate_acc), (up_w, up_acc)):
                product = jnp.dot(block, source[chunks[r]], preferred_element_type=jnp.float32)
                if r == 0:
                    acc[...] = product
                else:
                    acc[...] += product
        arrive("es", d)
        scale = lax.rsqrt(extra_columns(d, 0) / (4 * width) + epsilon)
        gate_value = gate_acc[...] * scale
        up_value = up_acc[...] * scale
        hidden[d, 0] = (gate_value / (1.0 + jnp.exp(-gate_value)) * up_value).astype(jnp.bfloat16)

    def spread_hidden(d):
        for k in range(2):
            part, rest = pl.ds(k * cap, cap), pl.ds((1 - k) * cap, cap)
            send(("hx", d, k), hidden.at[d, 0, part], hidden.at[d, 1, part], x_peer)
            send(("hy", d, k), hidden.at[d, 0, rest], hidden.at[d, 2, rest], y_peer)

    def relay_hidden(d):
        for k, axis, peer in ((0, "hx", y_peer), (1, "hy", x_peer)):
            arrive(axis, d, 0)
            part = pl.ds(k * cap, cap)
            send(("hvia", d, k), hidden.at[d, 1 + k, part], hidden.at[d, 3, part], peer)

    def finish(d):
        arrive("hx", d, 1)
        arrive("hy", d, 1)
        for r in range(4):
            if r == 3:
                arrive("hvia", d, 0)
                arrive("hvia", d, 1)
            product = jnp.dot(hidden[d, r], down_w[chunks[r]], preferred_element_type=jnp.float32)
            if r == 0:
                result[...] = product
            else:
                result[...] += product
        low, high = extra_columns(d, 1), extra_columns(d, 2)
        share = low + (high - low) * core.astype(jnp.float32)
        swap_send[d] = (result[cap:, :] * share[cap:]).astype(jnp.bfloat16)
        send(("swap", d), swap_send.at[d], swap_recv.at[d], sibling)
        kept = result[:cap, :] * share[:cap]
        arrive("swap", d)
        summed = (kept + swap_recv[d].astype(jnp.float32)).astype(jnp.bfloat16)
        if d == 0:
            arrived[pl.ds(0, cap)] = summed
            return
        back[d] = summed
        send(("back", d), back.at[d], arrived.at[pl.ds(d * cap, cap)], behind[d])

    rows[0, 0, pl.ds(0, cap)] = pick(0)
    spread(0)
    for d in range(1, chips):
        going[d] = pick(d)
        send(("z", d), going.at[d], slot_rows(d, 0), ahead[d])
    for r in range(1, 4):
        arrive("norm", r)
    norm_total = norms[0] + norms[1] + norms[2] + norms[3]
    table = jnp.where(line == 0, norm_total, routes[...])
    table_high = table.astype(jnp.bfloat16)
    table_low = (table - table_high.astype(jnp.float32)).astype(jnp.bfloat16)
    for d in range(chips):
        chosen = picker[pl.ds(d * cap, cap), :]
        picked = dot_nt(table_high, chosen) + dot_nt(table_low, chosen)
        picked = jnp.concatenate([picked, jnp.zeros((8, lanes - cap), jnp.float32)], axis=1)
        if d == 0:
            extras[0, 0] = picked
        else:
            norms_d = extras.at[2, d]
            extras[2, d] = picked
            send(("ez", d), norms_d, extras.at[0, d], ahead[d])
    extra_side(0)
    relay(0)
    spread(1)
    sides(0)
    extra_side(1)
    relay(1)
    spread(2)
    sides(1)
    for copy in gate_loads:
        copy.wait()
    project(0)
    relay(2)
    spread(3)
    sides(2)
    extra_side(2)
    project(1)
    spread_hidden(1)
    relay(3)
    sides(3)
    extra_side(3)
    project(2)
    relay_hidden(1)
    spread_hidden(2)
    project(3)
    relay_hidden(2)
    spread_hidden(3)
    down_load.wait()
    finish(1)
    relay_hidden(3)
    spread_hidden(0)
    finish(2)
    relay_hidden(0)
    finish(3)
    finish(0)
    for d in range(1, chips):
        arrive("back", d)
    final = jnp.dot(unpicker[...], arrived[...], preferred_element_type=jnp.float32)
    out_ref[...] = (stream[...] + final).astype(jnp.bfloat16)
    for copy in pending:
        copy.wait_send()


def rope_tables(sequence, count, heads, lean_size, broad_size):
    def angles(size):
        quarter = size // 4
        steps = np.arange(quarter, dtype=np.float32) / np.float32(quarter)
        frequency = np.float32(theta_base) ** (-steps)
        grid_rows = np.arange(sequence // GRID_W, dtype=np.float32)[:, None] * frequency
        grid_columns = np.arange(GRID_W, dtype=np.float32)[:, None] * frequency
        return grid_rows, grid_columns

    shards, per_shard = sequence // count, count // GRID_W
    row_angles, column_angles = angles(lean_size)
    lean_columns = np.tile(column_angles.T, (1, per_shard))
    lean_rows = np.repeat(row_angles, GRID_W, axis=0).reshape(shards, count, -1).transpose(0, 2, 1)
    lean = [
        np.concatenate([np.cos(lean_rows), np.sin(lean_rows)], axis=1),
        np.concatenate([np.cos(lean_columns), np.sin(lean_columns)], axis=0),
    ]
    row_angles, column_angles = angles(broad_size)

    def both(angle, first):
        blank = np.zeros_like(angle)
        cosine = [np.cos(angle), np.cos(angle)]
        sine = [-np.sin(angle), np.sin(angle)]
        rest = [blank, blank]
        parts = cosine + rest + sine + rest if first else rest + cosine + rest + sine
        return np.concatenate(parts, axis=1)

    broad_rows = both(row_angles, True).reshape(shards, per_shard, -1)
    broad_columns = np.repeat(both(column_angles, False), heads, axis=0)
    broad_columns = broad_columns.reshape(-1, 2, broad_size).transpose(1, 0, 2)
    return [table.astype(np.float32) for table in lean + [broad_rows, broad_columns]]


def paired_layer(
    chips,
    tokens,
    lean,
    lean_gains,
    broad,
    broad_gains,
    mixer_gain,
    output_weight,
    channel_gain,
    expert_weights,
    route_experts,
    route_logits,
    group_weight,
):
    count, width = tokens.shape
    heads, lean_size = lean[0].shape[1:]
    key_heads = lean[1].shape[1]
    broad_size = broad[0].shape[2]
    gate_weight, up_weight, down_weight = expert_weights
    ff = gate_weight.shape[1]
    cap = count // 2
    sequence = count * lax.axis_size("sp")
    tables = rope_tables(sequence, count, heads, lean_size, broad_size)
    operands = (
        [jnp.transpose(part, (1, 2, 0)) for part in lean]
        + [part.reshape(-1, broad_size) for part in broad]
        + [lean_gains, broad_gains]
        + [jnp.asarray(table) for table in tables]
        + [
            jnp.transpose(route_experts),
            jnp.transpose(route_logits),
            group_weight[None, :],
            mixer_gain[None, :],
            tokens,
            channel_gain[None, :],
            output_weight,
            gate_weight.reshape(4, width, ff),
            up_weight.reshape(4, width, ff),
            down_weight.reshape(4, ff, width),
        ]
    )
    landing = [part for part in operands]
    landing[8] = tables[0][0]
    landing[10] = tables[2][0]
    f32, bf16 = jnp.float32, jnp.bfloat16
    return pl.pallas_call(
        functools.partial(layer_kernel, chips),
        out_shape=jax.ShapeDtypeStruct((count, width), bf16),
        in_specs=[pl.BlockSpec(memory_space=pl.ANY)] * len(operands),
        out_specs=pl.BlockSpec(memory_space=pltpu.VMEM),
        scratch_shapes=[pltpu.VMEM(part.shape, part.dtype) for part in landing]
        + [
            pltpu.VMEM((2, count * key_heads, 128), f32),
            pltpu.VMEM((count, 384), bf16),
            pltpu.VMEM((chips, 2 * count, 384), bf16),
            pltpu.VMEM((2, count * heads, 128), bf16),
            pltpu.VMEM((2, count * heads, 128), f32),
            pltpu.VMEM((2, count * heads, 128), f32),
            pltpu.VMEM((count * heads, 128), f32),
            pltpu.VMEM((count * heads, 128), f32),
            pltpu.VMEM((4, count, heads * lean_size), bf16),
            pltpu.VMEM((4, count, heads * broad_size), bf16),
            pltpu.VMEM((count, width), f32),
            pltpu.VMEM((count, width), f32),
            pltpu.VMEM((count, width), f32),
            pltpu.VMEM((count, width), bf16),
            pltpu.VMEM((chips * cap, count), bf16),
            pltpu.VMEM((count, chips * cap), bf16),
            pltpu.VMEM((8, count), f32),
            pltpu.VMEM((4, 8, count), f32),
            pltpu.VMEM((3, chips, 8, 128), f32),
            pltpu.VMEM((chips, cap, width), bf16),
            pltpu.VMEM((chips, 4, 2 * cap, width), bf16),
            pltpu.VMEM((2 * cap, ff), f32),
            pltpu.VMEM((2 * cap, ff), f32),
            pltpu.VMEM((chips, 4, 2 * cap, ff), bf16),
            pltpu.VMEM((2 * cap, width), f32),
            pltpu.VMEM((chips, cap, width), bf16),
            pltpu.VMEM((chips, cap, width), bf16),
            pltpu.VMEM((chips, cap, width), bf16),
            pltpu.VMEM((chips * cap, width), bf16),
            pltpu.SemaphoreType.DMA((len(operands),)),
            pltpu.SemaphoreType.DMA((COPIES,)),
            pltpu.SemaphoreType.DMA((COPIES,)),
        ],
        compiler_params=pltpu.CompilerParams(
            collective_id=0, has_side_effects=True, vmem_limit_bytes=60 * 1024 * 1024
        ),
    )(*operands)


def on_device(
    tokens,
    lean_query,
    lean_key,
    lean_value,
    lean_gains,
    broad_query,
    broad_key,
    broad_value,
    broad_gains,
    mixer_gain,
    output_weight,
    channel_gain,
    gate_weight,
    up_weight,
    down_weight,
    route_experts,
    route_logits,
    group_weight,
):
    row_count = tokens.shape[0]
    positions = lax.axis_index("sp") * row_count + jnp.arange(row_count, dtype=jnp.int32)
    lane_index = lax.axis_index("tp")
    logit_gap = route_logits[:, 0] - route_logits[:, 1]
    weights = group_weight[:, None] * jax.nn.sigmoid(jnp.stack([logit_gap, -logit_gap], axis=1))
    chips = lax.axis_size("sp") // 2
    if (
        lax.axis_size("tp") == 4
        and chips == GROUPS
        and chips == 4
        and route_experts.shape[1] == 2
        and lean_query.shape[1:] == (4, 64)
        and broad_query.shape[1:] == (4, 128)
        and lean_key.shape[1:] == (2, 64)
        and broad_key.shape[1:] == (2, 128)
        and row_count % GRID_W == 0
    ):
        return paired_layer(
            chips,
            tokens,
            (lean_query, lean_key, lean_value),
            lean_gains,
            (broad_query, broad_key, broad_value),
            broad_gains,
            mixer_gain,
            output_weight,
            channel_gain,
            (gate_weight[0], up_weight[0], down_weight[0]),
            route_experts,
            route_logits,
            group_weight,
        )
    lean_queries, lean_keys, lean_values = own_heads(
        lean_query, lean_key, lean_value, lean_gains, positions, lane_index, HQ_A // KV_A
    )
    broad_queries, broad_keys, broad_values = own_heads(
        broad_query, broad_key, broad_value, broad_gains, positions, lane_index, HQ_B // KV_B
    )
    shard_rows = (
        lax.all_gather(lean_keys, "sp", axis=0, tiled=True),
        lax.all_gather(lean_values, "sp", axis=0, tiled=True),
        lax.all_gather(broad_keys, "sp", axis=0, tiled=True),
        lax.all_gather(broad_values, "sp", axis=0, tiled=True),
    )
    lean_state = attend_piece(start_state(lean_queries), lean_queries, shard_rows[0], shard_rows[1])
    broad_state = attend_piece(
        start_state(broad_queries), broad_queries, shard_rows[2], shard_rows[3]
    )
    lean_all, broad_all = (
        lax.all_gather(finish_heads(lean_state), "tp", axis=1, tiled=True),
        lax.all_gather(finish_heads(broad_state), "tp", axis=1, tiled=True),
    )
    lean_width = lean_all.shape[1]
    stream = tokens.astype(jnp.float32) + jnp.dot(
        group_norm(lean_all, mixer_gain[:lean_width]),
        output_weight[:lean_width],
        preferred_element_type=jnp.float32,
    )
    stream = stream + jnp.dot(
        group_norm(broad_all, mixer_gain[lean_width:]),
        output_weight[lean_width:],
        preferred_element_type=jnp.float32,
    )
    squares = lax.psum(jnp.sum(stream * stream, axis=1), "tp")
    normed = (stream * lax.rsqrt(squares / D + epsilon)[:, None] * channel_gain).astype(
        jnp.bfloat16
    )
    experts = lax.axis_size("sp")
    capacity = row_count // (experts // GROUPS)
    flat_experts = route_experts.reshape(-1)
    onehot = (flat_experts[:, None] == jnp.arange(experts, dtype=jnp.int32)[None, :]).astype(
        jnp.int32
    )
    slot_rank = jnp.sum((jnp.cumsum(onehot, axis=0) - 1) * onehot, axis=1)
    slot_index = flat_experts * capacity + slot_rank
    token_owner = jnp.repeat(jnp.arange(row_count, dtype=jnp.int32), route_experts.shape[1])
    filled = jnp.zeros((experts * capacity,), jnp.int32).at[slot_index].set(token_owner + 1)
    slot_live = (filled > 0)[:, None]
    source = jnp.maximum(filled - 1, 0)
    outgoing = jnp.where(slot_live, normed[source], jnp.zeros((), jnp.bfloat16)).reshape(
        experts, capacity, -1
    )
    arrived = lax.all_to_all(outgoing, "sp", split_axis=0, concat_axis=0, tiled=True)
    sources = arrived.shape[0]
    item_count = arrived.shape[1]
    shard_rows = lax.all_gather(arrived, "tp", axis=2, tiled=True)
    flat_rows = shard_rows.reshape(sources * item_count, shard_rows.shape[2])
    gate_part = gate_weight[0]
    up_part = up_weight[0]
    gate_value = jnp.dot(flat_rows, gate_part, preferred_element_type=jnp.float32)
    up_value = jnp.dot(flat_rows, up_part, preferred_element_type=jnp.float32)
    hidden = (jax.nn.silu(gate_value) * up_value).astype(jnp.bfloat16)
    down_part = down_weight[0]
    result = jnp.dot(
        lax.all_gather(hidden, "tp", axis=1, tiled=True),
        down_part,
        preferred_element_type=jnp.float32,
    )
    result = result.astype(jnp.bfloat16).reshape(sources, item_count, -1)
    returned = lax.all_to_all(result, "sp", split_axis=0, concat_axis=0, tiled=True)
    picked = (
        returned.reshape(experts * capacity, -1)[slot_index]
        .reshape(row_count, route_experts.shape[1], -1)
        .astype(jnp.float32)
    )
    return (stream + jnp.sum(picked * weights[:, :, None], axis=1)).astype(jnp.bfloat16)


def solution(mesh):
    return jax.shard_map(
        on_device,
        mesh=mesh,
        in_specs=(
            P("sp", "tp"),
            P("sp", "tp", None),
            P("sp", None, None),
            P("sp", None, None),
            P(),
            P("sp", "tp", None),
            P("sp", None, None),
            P("sp", None, None),
            P(),
            P(),
            P(None, "tp"),
            P("tp"),
            P("sp", None, "tp"),
            P("sp", None, "tp"),
            P("sp", None, "tp"),
            P("sp", None),
            P("sp", None),
            P("sp"),
        ),
        out_specs=P("sp", "tp"),
        check_vma=False,
    )
```

time: 136 us -> 110 us (0.81); the launches traced: 134 us -> 110 us
  Pallas kernels: 117 us -> 108 us
  local copies, waits for them, and re-layouts: 8.8 us -> 1.77 us
  other arithmetic: 5.46 us -> 0 us
  matrix products: 2.47 us -> 0 us
    pallas_call x2 -> x1, Pallas kernels: 117 us -> 108 us  [paired_layer(): pl.pallas_call(functools.partial(layer_kernel, chips), out_shape=jax.Shap...]
    reshape x4 -> x0, local copies, waits for them, and re-layouts: 3.87 us -> none  [run_front(): flat = [part.reshape(rows, -1) for part in lean + broad]]
    unnamed x11 -> x1, local copies, waits for them, and re-layouts: 4.93 us -> 1.77 us
    dot_general x2 -> x0, matrix products: 2.47 us -> none  [the longest x1 2.3 us: paired_block(): lax.dot_general(picker, arrived, (((0,), (0,)), ((), ())), preferred_elem...]
    mul x2 -> x0, other arithmetic: 2.17 us -> none  [the longest x1 1.48 us: run_front(): jnp.sin(angles) * sign]
where the time goes in v1:
time: 110 us
  Pallas kernels  108 us (98%)
  local copies, waits for them, and re-layouts  1.77 us (2%)
    pallas_call x1, Pallas kernels, paired_layer(): pl.pallas_call(functools.partial(layer_kernel, chips), out_shape=jax.Shap...  108 us

profile of v1, /device:TPU:0, one launch (start us, length us, event | category | flops | bytes accessed | tf_op | source)
XLA Modules:
  0.0 109.9 jit_solution(3300739457716926086)
XLA Ops:
  0.0 108.1 %shard_map.208 = bf16[192,1024]{1,0:T(8,128)(2,1)} custom-call(bf16[4,64,192]{2,1,0:T(8,128)(2,1)} %bitcast.18, bf16[2,64,192]{2,1,0:T(8,128)(2,1)} %bitcast.21, bf16[2,64,192]{2,1,0:T(8,128)(2,1)} %bitcast.22, bf16[768,128]{1,0:T(8,128)(2,1)} %bitcast.17, bf16[384,128]{1,0:T(8,128)(2,1)} %bitcast.19, bf16[384,128]{1,0:T(8,128)(2,1)} %bitcast.20, ...), custom_call_target="tpu_custom_call" | custom-call | tf_op jit(solution)/shard_map/pallas_call | solution.py:803
  108.1 1.8 %copy.24 = bf16[192,1024]{1,0:T(8,128)(2,1)} copy(bf16[192,1024]{1,0:T(8,128)(2,1)} %shard_map.208) | data formatting | bytes 786432
